TPU v7x, 256 devices: a 8x8x2 block of a 8x8x16 slice. The times are simulated.
256 devices in a mesh: grp: 2 (over z), ep: 16 (over y, core), tp: 8 (over x).
Axes of the slice: x: 8, y: 8, z: 2, core: 2. Of those that a mesh axis runs over, the one named last changes fastest.
The devices are a block of a 8x8x16 slice.
Arguments:
- tokens: bfloat16 [8192, 4096], P(('grp', 'ep')), parts along dimension 0, may hold values from -6 to 6
- expert_ids: int32 [8192, 2], P(('grp', 'ep')), parts along dimension 0, may hold values from 0 to 15, as said below
- gates: float32 [8192, 2], P(('grp', 'ep')), parts along dimension 0, may hold values from 0.1 to 1
- w_gate: bfloat16 [16, 4096, 2048], P('ep', None, 'tp'), may hold values from -0.09375 to 0.09375
- w_up: bfloat16 [16, 4096, 2048], P('ep', None, 'tp'), may hold values from -0.09375 to 0.09375
- w_down: bfloat16 [16, 2048, 4096], P('ep', 'tp'), may hold values from -0.79549513 to 0.79549513, as said below
- norm_gain: float32 [4096], P('tp'), may hold values from 0.1 to 1.9
- norm_bias: float32 [4096], P('tp'), may hold values from -1.5 to 1.5
Outputs:
- normed: bfloat16 [8192, 4096], P(('grp', 'ep'), 'tp'), parts along dimension 0
There are 2 independent parts, one for each index of `grp`. A program takes and returns all parts, laid end to end along the dimension named above; an argument that names none is the same for every part. Nothing has to cross between parts.
Inputs may be any that keep to these rules, and one draw needn't show every extreme that they name: `expert_ids`: each row names 2 different experts, both in the same group of 4 consecutive expert numbers. Within one aligned block of 256 rows no expert is named more than 64 times, and in every draw some expert is named exactly 64 times in every block. `w_down`: down projection weights.
All inputs are finite; a program needn't handle non-finite values.
Results may differ from a plain program's by a relative error of at most 0.014.
Values may be sent and summed in bfloat16 or wider, within the bound.
No kernel may reach another device: no remote copies, remote signals or barrier semaphores. Data moves between devices by JAX's collectives and lax.ppermute only.
A program may use at most 128 MiB of HBM per device.

v0:
```python
import jax
import jax.numpy as jnp
from jax import lax
from jax.sharding import PartitionSpec as P

D = 4096
TOPK = 2
EXPERTS = 16
CAP = 64
norm_eps = 1e-05


def copy_for_each(value, axis):
    peers = lax.axis_size(axis)
    return lax.all_to_all(
        jnp.broadcast_to(value[None], (peers, *value.shape)), axis, 0, 0, tiled=True
    )


def of_everyone(value, axis):
    everything = copy_for_each(value, axis)
    return jnp.sum(everything, axis=0)


def together(arrays, axis):
    ends = [0]
    for a in arrays:
        ends.append(ends[-1] + a.size)
    subtotal = of_everyone(jnp.concatenate([a.ravel() for a in arrays]), axis)
    return tuple((subtotal[b:e].reshape(a.shape) for a, b, e in zip(arrays, ends, ends[1:])))


def route_slots(expert_ids):
    flat_ids = expert_ids.reshape(-1)
    onehot = (flat_ids[:, None] == jnp.arange(EXPERTS, dtype=jnp.int32)[None, :]).astype(jnp.int32)
    position = jnp.sum((jnp.cumsum(onehot, axis=0) - 1) * onehot, axis=1)
    target = flat_ids * CAP + position
    token_of = jnp.arange(flat_ids.shape[0], dtype=jnp.int32) // TOPK
    source = jnp.zeros((EXPERTS * CAP,), jnp.int32).at[target].set(token_of)
    filled = jnp.zeros((EXPERTS * CAP,), jnp.bool_).at[target].set(True)
    return (target, source, filled)


def on_device(tokens, expert_ids, gates, w_gate, w_up, w_down, norm_gain, norm_bias):
    tok_rows, width = tokens.shape
    piece_width = norm_gain.shape[0]
    target, source, filled = route_slots(expert_ids)
    offset = lax.axis_index("tp") * piece_width
    own_columns = lax.dynamic_slice_in_dim(tokens, offset, piece_width, 1)
    outgoing = jnp.where(filled[:, None], own_columns[source], jnp.zeros((), jnp.bfloat16)).reshape(
        EXPERTS, CAP, piece_width
    )
    arrived = lax.all_to_all(outgoing, "ep", split_axis=0, concat_axis=1, tiled=True)
    segment = lax.all_gather(arrived, "tp", axis=2, tiled=True)
    gate_more = jnp.einsum("erd,edf->erf", segment, w_gate, preferred_element_type=jnp.float32)
    up_more = jnp.einsum("erd,edf->erf", segment, w_up, preferred_element_type=jnp.float32)
    hidden = (jax.nn.silu(gate_more) * up_more).astype(jnp.bfloat16)
    partial_value = jnp.einsum("erf,efd->erd", hidden, w_down, preferred_element_type=jnp.float32)
    summed = lax.psum_scatter(
        partial_value.astype(jnp.bfloat16), "tp", scatter_dimension=2, tiled=True
    )
    returned = lax.all_to_all(summed, "ep", split_axis=1, concat_axis=0, tiled=True)
    picked = returned.reshape(EXPERTS * CAP, piece_width)[target].reshape(
        tok_rows, TOPK, piece_width
    )
    combined = jnp.sum(picked.astype(jnp.float32) * gates[:, :, None], axis=1)
    stats = together((jnp.sum(combined, axis=1), jnp.sum(combined * combined, axis=1)), "tp")
    row_mean = stats[0] / D
    row_var = stats[1] / D - row_mean * row_mean
    normed = (combined - row_mean[:, None]) * lax.rsqrt(
        row_var[:, None] + norm_eps
    ) * norm_gain + norm_bias
    return normed.astype(jnp.bfloat16)


def solution(mesh):
    return jax.shard_map(
        on_device,
        mesh=mesh,
        in_specs=(
            P(("grp", "ep"), None),
            P(("grp", "ep"), None),
            P(("grp", "ep"), None),
            P("ep", None, "tp"),
            P("ep", None, "tp"),
            P("ep", "tp", None),
            P("tp"),
            P("tp"),
        ),
        out_specs=P(("grp", "ep"), "tp"),
        check_vma=False,
    )
```

profile of v0, /device:TPU:513, one launch (start us, length us, event | category | flops | bytes accessed | tf_op | source)
XLA Modules:
  0.0 358.6 jit_solution(16169199813096574413)
XLA Ops:
  6.6 1.0 copy.38
  8.5 1.2 reduce-window.6
  10.3 2.4 scatter_custom_fusion.1
  12.8 2.4 scatter_custom_fusion
  15.3 1.0 constant_dynamic-slice_fusion
  16.3 4.0 %gather_fusion = bf16[1024,512]{1,0:T(8,128)(2,1)S(1)} fusion(bf16[256,512]{1,0:T(8,128)(2,1)S(1)} %constant_dynamic-slice_fusion, s32[1024]{0:T(1024)S(1)} %fusion.20), kind=kCustom, calls=%fused_computation | custom fusion | bytes 2101248 | tf_op jit(solution)/shard_map/gather | solution.py:50
  20.5 52.0 %all_to_all.27 = bf16[16,64,512]{2,1,0:T(8,128)(2,1)} all-to-all(bf16[16,64,512]{2,1,0:T(8,128)(2,1)S(1)} %broadcast_select_fusion), channel_id=1, replica_groups=mesh['grp'=2,'ep'=16,'tp'=8] {'ep'}, dimensions={0} | all-to-all | bytes 2097152 | tf_op jit(solution)/shard_map/all_to_all | solution.py:53
  72.8 92.8 %all-gather.2.cloned.1.call-done = bf16[1,1024,4096]{2,1,0:T(8,128)(2,1)} async-done(((bf16[1,1024,512]{2,1,0:T(8,128)(2,1)}), bf16[1,1024,4096]{2,1,0:T(8,128)(2,1)}) %all-gather.2.cloned.1.call-update) | async-done | bytes 8388624 | tf_op jit(solution)/shard_map/all_gather | solution.py:54
  165.6 6.5 %fusion.2 = f32[1024,256]{1,0:T(8,128)S(1)} fusion(bf16[1,1024,4096]{2,1,0:T(8,128)(2,1)} %all-gather.2.cloned.1.call-done, bf16[1,4096,256]{2,1,0:T(8,128)(2,1)} %param.11), kind=kOutput, calls=%fused_computation.6 | convolution fusion | flops 2147483648 | bytes 11534336 | tf_op jit(solution)/shard_map/erd,edf->erf/dot_general | solution.py:55
  172.6 2.4 fusion.12
  174.9 5.6 %convert_bitcast_fusion = bf16[1,1024,4096]{2,1,0:T(8,128)(2,1)} fusion(bf16[1024,256]{1,0:T(8,128)(2,1)S(1)} %fusion.12, bf16[1,256,4096]{2,1,0:T(8,128)(2,1)S(1)} %copy-done), kind=kOutput, calls=%fused_computation.8 | convolution fusion | flops 2151677952 | bytes 11010048 | tf_op jit(solution)/shard_map/erf,efd->erd/dot_general | solution.py:58
  180.6 95.3 %reduce-scatter.2.cloned.1.call-done = bf16[1,1024,512]{2,1,0:T(8,128)(2,1)} async-done(((bf16[1,1024,4096]{2,1,0:T(8,128)(2,1)}), bf16[1,1024,512]{2,1,0:T(8,128)(2,1)}) %reduce-scatter.2.cloned.1.call-update) | async-done | bytes 1048592 | tf_op jit(solution)/shard_map/reduce_scatter | solution.py:59
  275.8 4.2 %copy.54 = bf16[1,1024,512]{2,0,1:T(2,128)(2,1)} copy(bf16[1,1024,512]{2,1,0:T(8,128)(2,1)} %reduce-scatter.2.cloned.1.call-done) | data formatting | bytes 2097152 | tf_op jit(solution)/shard_map/reduce_scatter | solution.py:59
  280.5 8.3 %reduce.6 = bf16[1024,512]{1,0:T(8,128)(2,1)S(1)} reduce(bf16[1024,1,512]{2,1,0:T(2,128)(2,1)} %bitcast.53, bf16[]{:T(256)} %broadcast.121), dimensions={1}, to_apply=%bitcast.50.reduce_sub_computation | reduce | bytes 2097154
  288.8 1.6 reshape.155
  290.4 7.7 %all-to-all-start.1 = ((bf16[16,2,16384]{2,1,0:T(2,128)(2,1)}), bf16[16,2,16384]{2,1,0:T(2,128)(2,1)S(1)}, u32[]{:S(2)}, u32[]{:S(2)}) async-start(bf16[16,2,16384]{2,1,0:T(2,128)(2,1)} %reshape.155), calls=%async_computation.2 | async-start | bytes 2097152 | tf_op jit(solution)/shard_map/all_to_all | solution.py:62
  298.4 27.7 %all-to-all-done.1 = bf16[16,2,16384]{2,1,0:T(2,128)(2,1)S(1)} async-done(((bf16[16,2,16384]{2,1,0:T(2,128)(2,1)}), bf16[16,2,16384]{2,1,0:T(2,128)(2,1)S(1)}, u32[]{:S(2)}, u32[]{:S(2)}) %all-to-all-start.1) | async-done | bytes 1048608 | tf_op jit(solution)/shard_map/all_to_all | solution.py:62
  326.1 3.5 reshape.156
  329.6 1.9 copy.53
  331.4 2.6 gather_fusion.1
  334.1 2.8 reshape.116
  336.8 2.6 multiply_reduce_fusion.1
  340.1 10.7 %all_to_all.28 = f32[8,1,512]{2,1,0:T(1,128)S(1)} all-to-all(f32[8,1,512]{2,1,0:T(1,128)S(1)} %broadcast_in_dim.45), channel_id=1, replica_groups=mesh['grp'=2,'ep'=16,'tp'=8] {'tp'}, dimensions={0} | all-to-all | bytes 32768 | tf_op jit(solution)/shard_map/all_to_all | solution.py:15
  350.9 0.9 add_convert_fusion
  (46 shorter events, 4.3 us)
Async XLA Ops:
  6.5 168.4 %copy-start = (bf16[1,256,4096]{2,1,0:T(8,128)(2,1)S(1)}, bf16[1,256,4096]{2,1,0:T(8,128)(2,1)}, u32[]{:S(2)}) copy-start(bf16[1,256,4096]{2,1,0:T(8,128)(2,1)} %param.13) | copy-start | bytes 6291460
  6.6 159.0 %all-gather.2.cloned.1.call-start = ((), (), s32[]{:S(2)}) async-start(), calls=%async_computation.4 | async-start | bytes 9437184 | tf_op jit(solution)/shard_map/all_gather | solution.py:54
  72.5 203.3 %reduce-scatter.2.cloned.1.call-start = ((), (), s32[]{:S(2)}) async-start(), calls=%async_computation.5 | async-start | bytes 9437184 | tf_op jit(solution)/shard_map/reduce_scatter | solution.py:59
  165.6 6.5 %copy-start.5 = (bf16[1,1024,4096]{2,1,0:T(8,128)(2,1)S(1)}, bf16[1,1024,4096]{2,1,0:T(8,128)(2,1)}, u32[]{:S(2)}) copy-start(bf16[1,1024,4096]{2,1,0:T(8,128)(2,1)} %all-gather.2.cloned.1.call-done) | copy-start | bytes 25165828
  165.6 7.0 %copy-start.6 = (bf16[1,4096,256]{2,1,0:T(8,128)(2,1)S(1)}, bf16[1,4096,256]{2,1,0:T(8,128)(2,1)}, u32[]{:S(2)}) copy-start(bf16[1,4096,256]{2,1,0:T(8,128)(2,1)} %param.12) | copy-start | bytes 6291460
  288.8 9.3 %copy-start.2 = (f32[256,2]{0,1:T(2,128)S(1)}, f32[256,2]{0,1:T(2,128)}, u32[]{:S(2)}) copy-start(f32[256,2]{0,1:T(2,128)} %param.10) | copy-start | bytes 6148
  290.4 35.7 %all-to-all-start.1 = ((bf16[16,2,16384]{2,1,0:T(2,128)(2,1)}), bf16[16,2,16384]{2,1,0:T(2,128)(2,1)S(1)}, u32[]{:S(2)}, u32[]{:S(2)}) async-start(bf16[16,2,16384]{2,1,0:T(2,128)(2,1)} %reshape.155), calls=%async_computation.2 | async-start | bytes 2097152 | tf_op jit(solution)/shard_map/all_to_all | solution.py:62
  334.1 5.5 %copy-start.1 = (bf16[512,512]{1,0:T(8,128)(2,1)S(1)}, bf16[512,512]{1,0:T(8,128)(2,1)}, u32[]{:S(2)}) copy-start(bf16[512,512]{1,0:T(8,128)(2,1)} %gather_fusion.1) | copy-start | bytes 1572868
  334.1 16.8 %copy-start.3 = (f32[512]{0:T(512)S(1)}, f32[512]{0:T(512)}, u32[]{:S(2)}) copy-start(f32[512]{0:T(512)} %param.15) | copy-start | bytes 6148
  334.1 16.8 %copy-start.4 = (f32[512]{0:T(512)S(1)}, f32[512]{0:T(512)}, u32[]{:S(2)}) copy-start(f32[512]{0:T(512)} %param.14) | copy-start | bytes 6148
Sparse Core Ops, SparseCore 0:
  72.7 92.8 all-gather.1
  180.7 95.0 reduce-scatter.1
where the time goes:
time: 359 us
  waiting for transfers between devices  216 us (60%)
  blocking collectives  62.7 us (17%)
  local copies, waits for them, and re-layouts  29.6 us (8%)
  other arithmetic  14.4 us (4%)
  matrix products  14.4 us (4%)
  between operations  13.7 us (4%)
  starting transfers between devices  7.98 us (2%)
    reduce_scatter x1, waiting for transfers between devices, on_device(): lax.psum_scatter(partial_value.astype(jnp.bfloat16), 'tp', scatter_dimens...  95.3 us
    all_gather x1, waiting for transfers between devices, on_device(): segment = lax.all_gather(arrived, 'tp', axis=2, tiled=True)  92.8 us
    all_to_all x1, blocking collectives, on_device(): lax.all_to_all(outgoing, 'ep', split_axis=0, concat_axis=1, tiled=True)  52 us
    all_to_all x1, waiting for transfers between devices, on_device(): lax.all_to_all(summed, 'ep', split_axis=1, concat_axis=0, tiled=True)  27.7 us
    all_to_all x1, blocking collectives, copy_for_each(): lax.all_to_all(jnp.broadcast_to(value[None], (peers, *value.shape)), axis...  10.7 us
    unnamed x20, local copies, waits for them, and re-layouts  9.03 us
    unnamed x1, other arithmetic  8.25 us
    all_to_all x1, starting transfers between devices, on_device(): lax.all_to_all(summed, 'ep', split_axis=1, concat_axis=0, tiled=True)  7.73 us
  transfers between devices with their start and end apart: 3, of which 3 were waited for; matrix products, arithmetic and copies ran while one was open for 0% of the time, Pallas kernels for 0%

commit v1 on v0

--- a/solution.py
+++ b/solution.py
@@ -2,6 +2,7 @@
 import jax.numpy as jnp
 from jax import lax
 from jax.sharding import PartitionSpec as P
+from jax.lax import all_to_all, psum
 
 D = 4096
 TOPK = 2
@@ -51,7 +52,13 @@
         EXPERTS, CAP, piece_width
     )
     arrived = lax.all_to_all(outgoing, "ep", split_axis=0, concat_axis=1, tiled=True)
-    segment = lax.all_gather(arrived, "tp", axis=2, tiled=True)
+
+    def bind_roads(local_block):
+        return jnp.concatenate(
+            all_to_all(jnp.stack([local_block] * psum(1, "tp"), 0), "tp", 0, 0), 2
+        )
+
+    segment = bind_roads(arrived)
     gate_more = jnp.einsum("erd,edf->erf", segment, w_gate, preferred_element_type=jnp.float32)
     up_more = jnp.einsum("erd,edf->erf", segment, w_up, preferred_element_type=jnp.float32)
     hidden = (jax.nn.silu(gate_more) * up_more).astype(jnp.bfloat16)

time: 359 us -> 451 us (1.26)
  blocking collectives: 62.7 us -> 251 us
  waiting for transfers between devices: 216 us -> 121 us
    all_to_all x0 -> x1, blocking collectives: none -> 189 us  [bind_roads(): all_to_all(jnp.stack([local_block] * psum(1, 'tp'), 0), 'tp', 0, 0)]
    all_gather x1 -> x0, waiting for transfers between devices: 92.8 us -> none  [on_device(): segment = lax.all_gather(arrived, 'tp', axis=2, tiled=True)]
  transfers between devices with their start and end apart: 3 -> 2, of which waited for: 3 -> 2; matrix products, arithmetic and copies ran while one was open for 0% -> 0% of each run, Pallas kernels for 0% -> 0%
where the time goes in v1:
time: 451 us; the launch traced here: 450 us
  blocking collectives  251 us (56%)
  waiting for transfers between devices  121 us (27%)
  local copies, waits for them, and re-layouts  31.7 us (7%)
  other arithmetic  14.4 us (3%)
  between operations  13.7 us (3%)
  matrix products  10.4 us (2%)
  starting transfers between devices  7.73 us (2%)
    all_to_all x1, blocking collectives, bind_roads(): all_to_all(jnp.stack([local_block] * psum(1, 'tp'), 0), 'tp', 0, 0)  189 us
    reduce_scatter x1, waiting for transfers between devices, on_device(): lax.psum_scatter(partial_value.astype(jnp.bfloat16), 'tp', scatter_dimens...  93.5 us
    all_to_all x1, blocking collectives, on_device(): lax.all_to_all(outgoing, 'ep', split_axis=0, concat_axis=1, tiled=True)  52 us
    all_to_all x1, waiting for transfers between devices, on_device(): lax.all_to_all(summed, 'ep', split_axis=1, concat_axis=0, tiled=True)  27.7 us
    all_to_all x1, blocking collectives, copy_for_each(): lax.all_to_all(jnp.broadcast_to(value[None], (peers, *value.shape)), axis...  10.7 us
  transfers between devices with their start and end apart: 2, of which 2 were waited for; matrix products, arithmetic and copies ran while one was open for 0% of the time, Pallas kernels for 0%

profile of v1, /device:TPU:513, one launch (start us, length us, event | category | flops | bytes accessed | tf_op | source)
XLA Modules:
  0.0 450.4 jit_solution(9942144403006005476)
XLA Ops:
  8.5 1.2 reduce-window.6
  10.3 2.4 scatter_custom_fusion.1
  12.8 2.4 scatter_custom_fusion
  15.3 1.0 constant_dynamic-slice_fusion
  16.3 4.0 gather_fusion
  20.5 52.0 %all_to_all.29 = bf16[16,64,512]{2,1,0:T(8,128)(2,1)} all-to-all(bf16[16,64,512]{2,1,0:T(8,128)(2,1)S(1)} %broadcast_select_fusion), channel_id=1, replica_groups=mesh['grp'=2,'ep'=16,'tp'=8] {'ep'}, dimensions={0} | all-to-all | bytes 2097152 | tf_op jit(solution)/shard_map/all_to_all | solution.py:54
  72.5 1.5 copy.48
  74.0 1.1 stack.5
  75.0 188.6 %all_to_all.30 = bf16[8,1,1024,512]{2,3,1,0:T(8,128)(2,1)S(1)} all-to-all(bf16[8,1,1024,512]{2,3,1,0:T(8,128)(2,1)S(1)} %stack.5), channel_id=1, replica_groups=mesh['grp'=2,'ep'=16,'tp'=8] {'tp'}, dimensions={0} | all-to-all | bytes 16777216 | tf_op jit(solution)/shard_map/all_to_all | solution.py:58
  263.6 2.4 fusion.3
  266.0 2.4 fusion.8
  268.4 5.6 %convert_bitcast_fusion = bf16[1,1024,4096]{2,1,0:T(8,128)(2,1)} fusion(bf16[1024,256]{1,0:T(8,128)(2,1)S(1)} %fusion.8, bf16[1,256,4096]{2,1,0:T(8,128)(2,1)S(1)} %copy-done), kind=kOutput, calls=%fused_computation.4 | convolution fusion | flops 2151677952 | bytes 11010048 | tf_op jit(solution)/shard_map/erf,efd->erd/dot_general | solution.py:65
  274.1 93.5 %reduce-scatter.2.cloned.1.call-done = bf16[1,1024,512]{2,1,0:T(8,128)(2,1)} async-done(((bf16[1,1024,4096]{2,1,0:T(8,128)(2,1)}), bf16[1,1024,512]{2,1,0:T(8,128)(2,1)}) %reduce-scatter.2.cloned.1.call-update) | async-done | bytes 1048592 | tf_op jit(solution)/shard_map/reduce_scatter | solution.py:66
  367.6 4.2 copy.63
  372.3 8.3 %reduce.6 = bf16[1024,512]{1,0:T(8,128)(2,1)S(1)} reduce(bf16[1024,1,512]{2,1,0:T(2,128)(2,1)} %bitcast.53, bf16[]{:T(256)} %broadcast.123), dimensions={1}, to_apply=%bitcast.48.reduce_sub_computation | reduce | bytes 2097154
  380.6 1.6 reshape.167
  382.2 7.7 %all-to-all-start.2 = ((bf16[16,2,16384]{2,1,0:T(2,128)(2,1)}), bf16[16,2,16384]{2,1,0:T(2,128)(2,1)S(1)}, u32[]{:S(2)}, u32[]{:S(2)}) async-start(bf16[16,2,16384]{2,1,0:T(2,128)(2,1)} %reshape.167), calls=%async_computation.3 | async-start | bytes 2097152 | tf_op jit(solution)/shard_map/all_to_all | solution.py:69
  390.2 27.7 %all-to-all-done.2 = bf16[16,2,16384]{2,1,0:T(2,128)(2,1)S(1)} async-done(((bf16[16,2,16384]{2,1,0:T(2,128)(2,1)}), bf16[16,2,16384]{2,1,0:T(2,128)(2,1)S(1)}, u32[]{:S(2)}, u32[]{:S(2)}) %all-to-all-start.2) | async-done | bytes 1048608 | tf_op jit(solution)/shard_map/all_to_all | solution.py:69
  417.9 3.5 reshape.168
  421.4 1.9 copy.62
  423.2 2.6 gather_fusion.1
  425.9 2.8 reshape.128
  428.6 2.6 multiply_reduce_fusion.1
  431.9 10.7 %all_to_all.31 = f32[8,1,512]{2,1,0:T(1,128)S(1)} all-to-all(f32[8,1,512]{2,1,0:T(1,128)S(1)} %broadcast_in_dim.45), channel_id=1, replica_groups=mesh['grp'=2,'ep'=16,'tp'=8] {'tp'}, dimensions={0} | all-to-all | bytes 32768 | tf_op jit(solution)/shard_map/all_to_all | solution.py:16
  (46 shorter events, 5.3 us)
Async XLA Ops:
  6.5 261.9 %copy-start = (bf16[1,256,4096]{2,1,0:T(8,128)(2,1)S(1)}, bf16[1,256,4096]{2,1,0:T(8,128)(2,1)}, u32[]{:S(2)}) copy-start(bf16[1,256,4096]{2,1,0:T(8,128)(2,1)} %param.13) | copy-start | bytes 6291460
  6.6 361.1 %reduce-scatter.2.cloned.1.call-start = ((), (), s32[]{:S(2)}) async-start(), calls=%async_computation.5 | async-start | bytes 9437184 | tf_op jit(solution)/shard_map/reduce_scatter | solution.py:66
  75.0 188.6 %copy-start.2 = (bf16[1,4096,256]{2,1,0:T(8,128)(2,1)S(1)}, bf16[1,4096,256]{2,1,0:T(8,128)(2,1)}, u32[]{:S(2)}) copy-start(bf16[1,4096,256]{2,1,0:T(8,128)(2,1)} %param.11) | copy-start | bytes 6291460
  263.6 2.4 copy-start.6
  380.6 9.3 %copy-start.3 = (f32[256,2]{0,1:T(2,128)S(1)}, f32[256,2]{0,1:T(2,128)}, u32[]{:S(2)}) copy-start(f32[256,2]{0,1:T(2,128)} %param.10) | copy-start | bytes 6148
  382.2 35.7 %all-to-all-start.2 = ((bf16[16,2,16384]{2,1,0:T(2,128)(2,1)}), bf16[16,2,16384]{2,1,0:T(2,128)(2,1)S(1)}, u32[]{:S(2)}, u32[]{:S(2)}) async-start(bf16[16,2,16384]{2,1,0:T(2,128)(2,1)} %reshape.167), calls=%async_computation.3 | async-start | bytes 2097152 | tf_op jit(solution)/shard_map/all_to_all | solution.py:69
  425.9 5.5 %copy-start.1 = (bf16[512,512]{1,0:T(8,128)(2,1)S(1)}, bf16[512,512]{1,0:T(8,128)(2,1)}, u32[]{:S(2)}) copy-start(bf16[512,512]{1,0:T(8,128)(2,1)} %gather_fusion.1) | copy-start | bytes 1572868
  425.9 16.8 %copy-start.4 = (f32[512]{0:T(512)S(1)}, f32[512]{0:T(512)}, u32[]{:S(2)}) copy-start(f32[512]{0:T(512)} %param.15) | copy-start | bytes 6148
  425.9 16.8 %copy-start.5 = (f32[512]{0:T(512)S(1)}, f32[512]{0:T(512)}, u32[]{:S(2)}) copy-start(f32[512]{0:T(512)} %param.14) | copy-start | bytes 6148
Sparse Core Ops, SparseCore 0:
  274.2 93.3 reduce-scatter.1
